TPU v7x, 32 devices: a whole 2x2x4 slice. The times are simulated.
32 devices in a mesh: sp: 4 (over z), fs: 4 (over y, x), tp: 2 (over core).
Axes of the slice: x: 2, y: 2, z: 4, core: 2. Of those that a mesh axis runs over, the one named last changes fastest.
Arguments:
- tokens: bfloat16 [8192, 2048], P(('fs', 'sp')), parts along dimension 0, may hold values from -6 to 6
- norm_gain: float32 [2048], replicated, may hold values from 0.1 to 1.9
- state_gate: bfloat16 [2048, 1024], P('sp', 'tp'), may hold values from -0.125 to 0.125
- state_value: bfloat16 [2048, 1024], P('sp', 'tp'), may hold values from -0.125 to 0.125
- state_keys: bfloat16 [2048, 1024], P('sp', 'tp'), may hold values from -0.125 to 0.125
- state_query: bfloat16 [2048, 1024], P('sp', 'tp'), may hold values from -0.125 to 0.125
- state_step: bfloat16 [2048, 16], replicated, may hold values from -0.125 to 0.125
- state_rate: float32 [16], P('tp'), may hold values from 0 to 1, as said below
- state_jumps: float32 [8192, 16], P(('fs', 'sp'), 'tp'), parts along dimension 0, may hold values from -3 to 0
- state_gain: float32 [1024], P('tp'), may hold values from 0.1 to 1.9
- filter_value: bfloat16 [5, 1024], P(None, 'tp'), may hold values from -2.5 to 2.5
- filter_keys: bfloat16 [5, 1024], P(None, 'tp'), may hold values from -2.5 to 2.5
- filter_query: bfloat16 [5, 1024], P(None, 'tp'), may hold values from -2.5 to 2.5
- window_query: bfloat16 [2048, 2048], P('sp', 'tp'), may hold values from -64 to 64
- window_keys: bfloat16 [2048, 1024], P('sp', 'tp'), may hold values from -1 to 1
- window_values: bfloat16 [2048, 1024], P('sp', 'tp'), may hold values from -0.125 to 0.125
- window_sink: float32 [16], P('tp'), may hold values from 2.5 to 5.5
- state_output: bfloat16 [1024, 2048], P('tp', 'sp'), may hold values from -0.1875 to 0.1875
- window_output: bfloat16 [2048, 2048], P('tp', 'sp'), may hold values from -2 to 2
Outputs:
- mixed: bfloat16 [8192, 2048], P(('fs', 'sp', 'tp')), parts along dimension 0
There are 4 independent parts, one for each index of `fs`. A program takes and returns all parts, laid end to end along the dimension named above; an argument that names none is the same for every part. Nothing has to cross between parts.
Inputs may be any that keep to these rules, and one draw needn't show every extreme that they name: `state_rate`: a positive rate for each head.
All inputs are finite; a program needn't handle non-finite values.
Results may differ from a plain program's by a relative error of at most 0.015.
The roundings to bfloat16 on the way count: a program that leaves them out, or rounds other values in their place, can miss the bound.
Values may be sent and summed in bfloat16 or wider, within the bound.
A program may use at most 64 MiB of HBM per device.

v0:
```python
import jax
import jax.numpy as jnp
from jax import lax
from jax.sharding import PartitionSpec as P

STATE_SIZE = 128
HEAD_DIM = 128
WINDOW = 128
BLOCK = 128
GRID_WIDTH = 64


def extended(cells, sides, width):
    for axis, dim in sides:
        count = lax.axis_size(axis)
        ends = count - 1
        head = lax.slice_in_dim(cells, 0, width, axis=dim)
        tail = lax.slice_in_dim(cells, cells.shape[dim] - width, cells.shape[dim], axis=dim)
        cells = jnp.concatenate(
            [
                lax.ppermute(tail, axis, [(i, (i + 1) % count) for i in range(ends)]),
                cells,
                lax.ppermute(head, axis, [((i + 1) % count, i) for i in range(ends)]),
            ],
            axis=dim,
        )
    return cells


def rotate_grid(vectors, positions, grid_width):
    head_dim = vectors.shape[-1]
    quarter = head_dim // 4
    half_dim = head_dim // 2
    inverse = 10000.0 ** (-jnp.arange(quarter, dtype=jnp.float32) / quarter)
    grid_row = (positions // grid_width).astype(jnp.float32)
    grid_col = (positions % grid_width).astype(jnp.float32)
    angle_row = grid_row[:, None] * inverse[None, :]
    angle_col = grid_col[:, None] * inverse[None, :]
    angles = jnp.concatenate([angle_row, angle_row, angle_col, angle_col], axis=-1)[:, None, :]
    first_half = vectors[..., :half_dim]
    second = vectors[..., half_dim:]
    turned = jnp.concatenate(
        [
            -first_half[..., quarter:],
            first_half[..., :quarter],
            -second[..., quarter:],
            second[..., :quarter],
        ],
        axis=-1,
    )
    return (
        vectors.astype(jnp.float32) * jnp.cos(angles) + turned.astype(jnp.float32) * jnp.sin(angles)
    ).astype(jnp.bfloat16)


def window_attend(query_rows, keys_pad, values_pad, sink_logits, key_start, total_len, window):
    row_count, query_heads, head_dim = query_rows.shape
    kv_heads = keys_pad.shape[1]
    group_size = query_heads // kv_heads
    block_count = row_count // window
    query_blocks = query_rows.reshape(block_count, window, kv_heads, group_size, head_dim)
    key_split = keys_pad.reshape(block_count + 2, window, kv_heads, head_dim)
    value_split = values_pad.reshape(block_count + 2, window, kv_heads, head_dim)
    key_band = jnp.concatenate([key_split[:-2], key_split[1:-1], key_split[2:]], axis=1)
    value_band = jnp.concatenate([value_split[:-2], value_split[1:-1], value_split[2:]], axis=1)
    scores = jnp.einsum(
        "kihgd,kjhd->khgij", query_blocks, key_band, preferred_element_type=jnp.float32
    ) * head_dim ** (-0.5)
    query_pos = jnp.arange(window)[:, None]
    band_pos = jnp.arange(3 * window)[None, :]
    within = jnp.abs(band_pos - window - query_pos) <= window
    key_pos = (
        key_start + jnp.arange(block_count)[:, None] * window + jnp.arange(3 * window)[None, :]
    )
    inside = (key_pos >= 0) & (key_pos < total_len)
    valid_pair = (within[None] & inside[:, None, :])[:, None, None]
    sink_logit = sink_logits.reshape(kv_heads, group_size)[None, :, :, None, None]
    masked = jnp.where(valid_pair, scores, -1e30)
    ceiling = jnp.maximum(jnp.max(masked, axis=-1, keepdims=True), sink_logit)
    weights = jnp.where(valid_pair, jnp.exp(masked - ceiling), 0.0)
    denominator = jnp.exp(sink_logit - ceiling) + jnp.sum(weights, axis=-1, keepdims=True)
    weights_bf = (weights / denominator).astype(jnp.bfloat16)
    mixed_rows = jnp.einsum(
        "khgij,kjhd->kihgd", weights_bf, value_band, preferred_element_type=jnp.float32
    )
    return mixed_rows.reshape(row_count, query_heads * head_dim).astype(jnp.bfloat16)


def block_terms(query_rows, key_rows, value_rows, log_rows, block_len):
    row_count, group_count, state_size = query_rows.shape
    head_ratio, head_dim = (value_rows.shape[2], value_rows.shape[3])
    block_count = row_count // block_len
    query_blocks = query_rows.reshape(block_count, block_len, group_count, state_size)
    key_blocks = key_rows.reshape(block_count, block_len, group_count, state_size)
    value_blocks = value_rows.reshape(block_count, block_len, group_count, head_ratio, head_dim)
    decay_cum = jnp.cumsum(
        log_rows.reshape(block_count, block_len, group_count, head_ratio), axis=1
    )
    decay_total = decay_cum[:, -1]
    gram_block = jnp.einsum(
        "kign,kjgn->kgij", query_blocks, key_blocks, preferred_element_type=jnp.float32
    )
    cum_heads = jnp.moveaxis(decay_cum, 1, 3)
    distance = jnp.abs(cum_heads[..., :, None] - cum_heads[..., None, :])
    pair_weight = (gram_block[:, :, None] * jnp.exp(-distance)).astype(jnp.bfloat16)
    near_terms = jnp.einsum(
        "kgrij,kjgrp->kigrp", pair_weight, value_blocks, preferred_element_type=jnp.float32
    )
    keys_after = (
        key_blocks[:, :, :, None, :] * jnp.exp(decay_total[:, None] - decay_cum)[..., None]
    ).astype(jnp.bfloat16)
    keys_before = (key_blocks[:, :, :, None, :] * jnp.exp(decay_cum)[..., None]).astype(
        jnp.bfloat16
    )
    state_after = jnp.einsum(
        "kjgrn,kjgrp->kgrnp", keys_after, value_blocks, preferred_element_type=jnp.float32
    )
    state_before = jnp.einsum(
        "kjgrn,kjgrp->kgrnp", keys_before, value_blocks, preferred_element_type=jnp.float32
    )
    before = jnp.cumsum(decay_total, axis=0) - decay_total
    overall = jnp.sum(decay_total, axis=0)
    after_sum = overall[None] - before - decay_total
    block_order = jnp.arange(block_count)
    earlier_mask = (block_order[None, :] < block_order[:, None])[:, :, None, None]
    later_mask = (block_order[None, :] > block_order[:, None])[:, :, None, None]
    gap_fwd = before[:, None] - before[None, :] - decay_total[None, :]
    gap_bwd = before[None, :] - before[:, None] - decay_total[:, None]
    weight_fwd = jnp.where(earlier_mask, jnp.exp(jnp.minimum(gap_fwd, 0.0)), 0.0)
    weight_bwd = jnp.where(later_mask, jnp.exp(jnp.minimum(gap_bwd, 0.0)), 0.0)
    carried_fwd = jnp.einsum(
        "abgr,bgrnp->agrnp", weight_fwd, state_after, precision=lax.Precision.HIGHEST
    )
    carried_bwd = jnp.einsum(
        "abgr,bgrnp->agrnp", weight_bwd, state_before, precision=lax.Precision.HIGHEST
    )
    summary_fwd = jnp.einsum(
        "agr,agrnp->grnp", jnp.exp(after_sum), state_after, precision=lax.Precision.HIGHEST
    )
    summary_bwd = jnp.einsum(
        "agr,agrnp->grnp", jnp.exp(before), state_before, precision=lax.Precision.HIGHEST
    )
    pieces = (
        near_terms,
        carried_fwd,
        carried_bwd,
        decay_cum,
        decay_total,
        before,
        after_sum,
        query_blocks,
    )
    return (pieces, (summary_fwd, summary_bwd, overall))


def finish_terms(pieces, incoming_fwd, incoming_bwd):
    (
        near_terms,
        carried_fwd,
        carried_bwd,
        decay_cum,
        decay_total,
        before,
        after_sum,
        query_blocks,
    ) = pieces
    total_fwd = carried_fwd + jnp.exp(before)[..., None, None] * incoming_fwd[None]
    total_bwd = carried_bwd + jnp.exp(after_sum)[..., None, None] * incoming_bwd[None]
    query_wide = query_blocks.astype(jnp.float32)
    read_fwd = jnp.einsum(
        "kign,kgrnp->kigrp", query_wide, total_fwd, precision=lax.Precision.HIGHEST
    )
    read_bwd = jnp.einsum(
        "kign,kgrnp->kigrp", query_wide, total_bwd, precision=lax.Precision.HIGHEST
    )
    combined = (
        near_terms
        + jnp.exp(decay_cum)[..., None] * read_fwd
        + jnp.exp(decay_total[:, None] - decay_cum)[..., None] * read_bwd
    )
    block_count, block_len, group_count, head_ratio, head_dim = combined.shape
    return combined.reshape(block_count * block_len, group_count, head_ratio, head_dim)


def combine_all(gathered_states, own_index):
    after_all, before_all, logs_all = gathered_states
    device_count = logs_all.shape[0]
    cum_incl = jnp.cumsum(logs_all, axis=0)
    cum_excl = cum_incl - logs_all
    device_order = jnp.arange(device_count)
    picker = (device_order == own_index).astype(jnp.float32)[:, None, None]
    own_incl = jnp.sum(picker * cum_incl, axis=0)
    own_excl = jnp.sum(picker * cum_excl, axis=0)
    lower_mask = (device_order < own_index)[:, None, None]
    higher_mask = (device_order > own_index)[:, None, None]
    weight_fwd = jnp.where(lower_mask, jnp.exp(jnp.minimum(own_excl[None] - cum_incl, 0.0)), 0.0)
    weight_bwd = jnp.where(higher_mask, jnp.exp(jnp.minimum(cum_excl - own_incl[None], 0.0)), 0.0)
    incoming_fwd = jnp.einsum(
        "dgr,dgrnp->grnp", weight_fwd, after_all, precision=lax.Precision.HIGHEST
    )
    incoming_bwd = jnp.einsum(
        "dgr,dgrnp->grnp", weight_bwd, before_all, precision=lax.Precision.HIGHEST
    )
    return (incoming_fwd, incoming_bwd)


def shards(
    tokens,
    norm_gain,
    state_gate,
    state_value,
    state_keys,
    state_query,
    state_step,
    state_rate,
    state_jumps,
    state_gain,
    filter_value,
    filter_keys,
    filter_query,
    window_query,
    window_keys,
    window_values,
    window_sink,
    state_output,
    window_output,
):
    row_count = tokens.shape[0]
    rows_wide = tokens.astype(jnp.float32)
    normed = (
        rows_wide
        * lax.rsqrt(jnp.mean(rows_wide * rows_wide, axis=-1, keepdims=True) + 1e-06)
        * norm_gain
    ).astype(jnp.bfloat16)
    gathered = (
        lax.all_gather(state_gate, "sp", axis=0, tiled=True),
        lax.all_gather(state_value, "sp", axis=0, tiled=True),
        lax.all_gather(state_keys, "sp", axis=0, tiled=True),
        lax.all_gather(state_query, "sp", axis=0, tiled=True),
        lax.all_gather(window_query, "sp", axis=0, tiled=True),
        lax.all_gather(window_keys, "sp", axis=0, tiled=True),
        lax.all_gather(window_values, "sp", axis=0, tiled=True),
        lax.all_gather(state_output, "sp", axis=1, tiled=True),
        lax.all_gather(window_output, "sp", axis=1, tiled=True),
    )
    projected = [
        jnp.dot(normed, matrix, preferred_element_type=jnp.float32) for matrix in gathered[:7]
    ]
    out_state = gathered[7]
    out_window = gathered[8]
    gate_rows, value_pre, keys_pre, query_pre, query_raw, keys_raw, values_rows = [
        result.astype(jnp.bfloat16) for result in projected
    ]
    head_local = state_rate.shape[0]
    group_local = keys_pre.shape[1] // STATE_SIZE
    head_dim = value_pre.shape[1] // head_local
    head_ratio = head_local // group_local
    step_cols = lax.dynamic_slice_in_dim(
        state_step, lax.axis_index("tp") * head_local, head_local, 1
    )
    step_rows = jax.nn.softplus(jnp.dot(normed, step_cols, preferred_element_type=jnp.float32))
    log_decay = -state_rate[None, :] * step_rows + state_jumps
    half_width = filter_value.shape[0] // 2
    stacked = jnp.concatenate([value_pre, keys_pre, query_pre], axis=-1)
    padded = extended(stacked, (("sp", 0),), half_width)
    filters = jnp.concatenate([filter_value, filter_keys, filter_query], axis=-1).astype(
        jnp.float32
    )
    filtered = jnp.zeros(stacked.shape, jnp.float32)
    for offset in range(filters.shape[0]):
        filtered = (
            filtered + padded[offset : offset + row_count].astype(jnp.float32) * filters[offset]
        )
    value_cols = value_pre.shape[1]
    key_cols = keys_pre.shape[1]
    inner_rows = (
        jax.nn.silu(filtered[:, :value_cols]).reshape(row_count, head_local, head_dim)
        * step_rows[..., None]
    )
    scan_values = inner_rows.astype(jnp.bfloat16).reshape(
        row_count, group_local, head_ratio, head_dim
    )
    scan_keys = (
        filtered[:, value_cols : value_cols + key_cols]
        .astype(jnp.bfloat16)
        .reshape(row_count, group_local, STATE_SIZE)
    )
    scan_query = (
        filtered[:, value_cols + key_cols :]
        .astype(jnp.bfloat16)
        .reshape(row_count, group_local, STATE_SIZE)
    )
    pieces, summaries = block_terms(
        scan_query,
        scan_keys,
        scan_values,
        log_decay.reshape(row_count, group_local, head_ratio),
        BLOCK,
    )
    summary_fwd, summary_bwd, overall = summaries
    gathered_states = (
        lax.all_gather(summary_fwd[None].astype(jnp.bfloat16), "sp", axis=0, tiled=True).astype(
            jnp.float32
        ),
        lax.all_gather(summary_bwd[None].astype(jnp.bfloat16), "sp", axis=0, tiled=True).astype(
            jnp.float32
        ),
        lax.all_gather(overall[None].astype(jnp.bfloat16), "sp", axis=0, tiled=True).astype(
            jnp.float32
        ),
    )
    incoming_fwd, incoming_bwd = combine_all(gathered_states, lax.axis_index("sp"))
    scan_out = finish_terms(pieces, incoming_fwd, incoming_bwd).reshape(
        row_count, head_local * head_dim
    )
    gated_rows = scan_out * jax.nn.silu(gate_rows.astype(jnp.float32))
    per_head = gated_rows.reshape(row_count, head_local, head_dim)
    state_mix = (
        (
            per_head
            * lax.rsqrt(jnp.mean(per_head * per_head, axis=-1, keepdims=True) + 1e-06)
            * state_gain.reshape(head_local, head_dim)
        )
        .astype(jnp.bfloat16)
        .reshape(row_count, head_local * head_dim)
    )
    query_heads = window_sink.shape[0]
    kv_heads = keys_raw.shape[1] // HEAD_DIM
    kv_width = kv_heads * HEAD_DIM
    positions = lax.axis_index("sp") * row_count + jnp.arange(row_count, dtype=jnp.int32)
    query_rot = rotate_grid(
        query_raw.reshape(row_count, query_heads, HEAD_DIM), positions, GRID_WIDTH
    )
    keys_rot = rotate_grid(keys_raw.reshape(row_count, kv_heads, HEAD_DIM), positions, GRID_WIDTH)
    pair_rows = jnp.concatenate([keys_rot.reshape(row_count, kv_width), values_rows], axis=-1)
    padded_pair = extended(pair_rows, (("sp", 0),), WINDOW)
    keys_pad = padded_pair[:, :kv_width].reshape(-1, kv_heads, HEAD_DIM)
    values_pad = padded_pair[:, kv_width:].reshape(-1, kv_heads, HEAD_DIM)
    window_mix = window_attend(
        query_rot,
        keys_pad,
        values_pad,
        window_sink,
        lax.axis_index("sp") * row_count - WINDOW,
        lax.axis_size("sp") * row_count,
        WINDOW,
    )
    return lax.psum_scatter(
        (
            jnp.dot(state_mix, out_state, preferred_element_type=jnp.float32)
            + jnp.dot(window_mix, out_window, preferred_element_type=jnp.float32)
        ).astype(jnp.bfloat16),
        "tp",
        scatter_dimension=0,
        tiled=True,
    )


def solution(mesh):
    placed = (
        P(("fs", "sp"), None),
        P(),
        P("sp", "tp"),
        P("sp", "tp"),
        P("sp", "tp"),
        P("sp", "tp"),
        P(),
        P("tp"),
        P(("fs", "sp"), "tp"),
        P("tp"),
        P(None, "tp"),
        P(None, "tp"),
        P(None, "tp"),
        P("sp", "tp"),
        P("sp", "tp"),
        P("sp", "tp"),
        P("tp"),
        P("tp", "sp"),
        P("tp", "sp"),
    )
    return jax.shard_map(
        shards, mesh=mesh, in_specs=placed, out_specs=P(("fs", "sp", "tp"), None), check_vma=False
    )
```

profile of v0, /device:TPU:0, one launch (start us, length us, event | category | flops | bytes accessed | tf_op | source)
XLA Modules:
  0.0 539.9 jit_solution(15252986102147311242)
XLA Ops:
  20.1 13.3 %all-gather.3 = bf16[4,4,2]{1,2,0:T(2,128)(2,1)S(1)} all-gather(bf16[1,4,2]{1,2,0:T(2,128)(2,1)S(1)} %convert_bitcast_fusion), channel_id=2, replica_groups=mesh['sp'=4,'fs'=4,'tp'=2] {'sp'}, dimensions={0}, use_global_device_ids=true | all-gather | bytes 80 | tf_op jit(solution)/shard_map/all_gather | solution.py:308
  40.1 17.2 %all-gather.24.cloned.1.call-done = bf16[2048,512]{1,0:T(8,128)(2,1)} async-done(((bf16[512,512]{1,0:T(8,128)(2,1)}), bf16[2048,512]{1,0:T(8,128)(2,1)}) %all-gather.24.cloned.1.call-update) | async-done | bytes 2097168 | tf_op jit(solution)/shard_map/all_gather | solution.py:241
  57.4 3.0 convolution_convert_fusion.2
  60.4 43.0 %all-gather.18.cloned.1.call-done = bf16[2048,512]{1,0:T(8,128)(2,1)} async-done(((bf16[512,512]{1,0:T(8,128)(2,1)}), bf16[2048,512]{1,0:T(8,128)(2,1)}) %all-gather.18.cloned.1.call-update) | async-done | bytes 2097168 | tf_op jit(solution)/shard_map/all_gather | solution.py:239
  103.4 3.6 convolution_convert_fusion.4
  107.0 42.5 %all-gather.16.cloned.1.call-done = bf16[2048,512]{1,0:T(8,128)(2,1)} async-done(((bf16[512,512]{1,0:T(8,128)(2,1)}), bf16[2048,512]{1,0:T(8,128)(2,1)}) %all-gather.16.cloned.1.call-update) | async-done | bytes 2097168 | tf_op jit(solution)/shard_map/all_gather | solution.py:238
  149.5 3.6 convolution_convert_fusion.5
  153.1 42.3 %all-gather.14.cloned.1.call-done = bf16[2048,512]{1,0:T(8,128)(2,1)} async-done(((bf16[512,512]{1,0:T(8,128)(2,1)}), bf16[2048,512]{1,0:T(8,128)(2,1)}) %all-gather.14.cloned.1.call-update) | async-done | bytes 2097168 | tf_op jit(solution)/shard_map/all_gather | solution.py:237
  195.4 3.6 convolution_convert_fusion.6
  200.2 2.8 collective-permute-start
  205.2 44.7 %all-gather.26.cloned.1.call-done = bf16[2048,512]{1,0:T(8,128)(2,1)} async-done(((bf16[512,512]{1,0:T(8,128)(2,1)}), bf16[2048,512]{1,0:T(8,128)(2,1)}) %all-gather.26.cloned.1.call-update) | async-done | bytes 2097168 | tf_op jit(solution)/shard_map/all_gather | solution.py:242
  249.9 3.6 convolution_convert_fusion.1
  255.4 2.0 collective-permute-start.2
  258.7 2.1 copy.213
  261.8 5.9 %maximum_maximum_fusion = (bf16[514,1536]{0,1:T(8,128)(2,1)S(1)}, bf16[514,1536]{0,1:T(8,128)(2,1)S(1)}) fusion(bf16[512,512]{0,1:T(8,128)(2,1)S(1)} %convolution_convert_fusion.4, bf16[512,512]{0,1:T(8,128)(2,1)S(1)} %convolution_convert_fusion.5, bf16[512,512]{0,1:T(8,128)(2,1)S(1)} %convolution_convert_fusion.6, bf16[2,1536]{0,1:T(8,128)(2,1)} %collective-permute-done, ...), kind=kLoop, calls=%fused_computation.19 | loop fusion | flops 12632064 | bytes 4743168 | tf_op jit(solution)/shard_map/concatenate | solution.py:19
  267.7 5.8 %fusion.122 = (bf16[512,1536]{0,1:T(8,128)(2,1)}, f32[512,1536]{0,1:T(8,128)S(1)}) fusion(f32[1536]{0:T(1024)S(1)} %get-tuple-element.9, bf16[514,1536]{0,1:T(8,128)(2,1)S(1)} %get-tuple-element.19, f32[1536]{0:T(1024)S(1)} %get-tuple-element.6, f32[1536]{0:T(1024)S(1)} %get-tuple-element.7, bf16[512,512]{0,1:T(8,128)(2,1)S(1)} %convolution_convert_fusion.4, ...), kind=kLoop, calls=%fused_computation.221 | loop fusion | flops 15728640 | bytes 12613632 | tf_op jit(solution)/shard_map/convert.2
  274.7 2.5 reshape.409
  284.0 23.4 %all-gather.1 = bf16[16,2,128,64]{2,3,1,0:T(8,128)(2,1)S(1)} all-gather(bf16[4,2,128,64]{2,3,1,0:T(8,128)(2,1)S(1)} %get-tuple-element.59), channel_id=3, replica_groups=mesh['sp'=4,'fs'=4,'tp'=2] {'sp'}, dimensions={0}, use_global_device_ids=true | all-gather | bytes 655360 | tf_op jit(solution)/shard_map/all_gather | solution.py:302
  308.5 16.1 %all-gather.2 = bf16[16,2,128,64]{2,3,1,0:T(8,128)(2,1)S(1)} all-gather(bf16[4,2,128,64]{2,3,1,0:T(8,128)(2,1)S(1)} %get-tuple-element.62), channel_id=4, replica_groups=mesh['sp'=4,'fs'=4,'tp'=2] {'sp'}, dimensions={0}, use_global_device_ids=true | all-gather | bytes 655360 | tf_op jit(solution)/shard_map/all_gather | solution.py:305
  326.3 2.6 fusion.20
  330.2 2.7 fusion.19
  334.8 3.9 bitcast_reduce_fusion
  346.6 45.2 %all-gather.28.cloned.1.call-done = bf16[2048,1024]{1,0:T(8,128)(2,1)} async-done(((bf16[512,1024]{1,0:T(8,128)(2,1)}), bf16[2048,1024]{1,0:T(8,128)(2,1)}) %all-gather.28.cloned.1.call-update) | async-done | bytes 4194320 | tf_op jit(solution)/shard_map/all_gather | solution.py:240
  391.8 5.4 %convolution_convert_fusion = bf16[512,1024]{1,0:T(8,128)(2,1)S(1)} fusion(bf16[2048,1024]{1,0:T(8,128)(2,1)} %all-gather.28.cloned.1.call-done, bf16[512,2048]{1,0:T(8,128)(2,1)} %param.19, f32[2048]{0:T(1024)S(1)} %copy-done.23, f32[512]{0:T(512)S(1)} %copy-done.17), kind=kOutput, calls=%fused_computation.34 | convolution fusion | flops 2152202240 | bytes 7350272 | tf_op jit(solution)/shard_map/dot_general | solution.py:247
  397.2 3.1 reshape.412
  408.4 5.3 fusion
  415.7 2.3 fusion.18
  419.9 52.7 %all-gather.30.cloned.1.call-done = bf16[1024,2048]{1,0:T(8,128)(2,1)} async-done(((bf16[1024,512]{1,0:T(8,128)(2,1)}), bf16[1024,2048]{1,0:T(8,128)(2,1)}) %all-gather.30.cloned.1.call-update) | async-done | bytes 4194320 | tf_op jit(solution)/shard_map/all_gather | solution.py:244
  472.6 6.5 %fusion.128 = f32[512,2048]{1,0:T(8,128)} fusion(bf16[512,1024]{1,0:T(8,128)(2,1)S(1)} %convert_element_type.224, bf16[1024,2048]{1,0:T(8,128)(2,1)} %all-gather.30.cloned.1.call-done), kind=kOutput, calls=%fused_computation.227 | convolution fusion | flops 2147483648 | bytes 9437184 | tf_op jit(solution)/shard_map/dot_general | solution.py:351
  479.2 39.2 %all-gather.22.cloned.1.call-done = bf16[512,2048]{1,0:T(8,128)(2,1)} async-done(((bf16[512,512]{1,0:T(8,128)(2,1)}), bf16[512,2048]{1,0:T(8,128)(2,1)}) %all-gather.22.cloned.1.call-update) | async-done | bytes 2097168 | tf_op jit(solution)/shard_map/all_gather | solution.py:243
  518.4 5.5 %add_convert_fusion = bf16[512,2048]{1,0:T(8,128)(2,1)} fusion(f32[512,2048]{1,0:T(8,128)} %fusion.128, bf16[512,512]{0,1:T(8,128)(2,1)S(1)} %fusion.41, bf16[512,2048]{1,0:T(8,128)(2,1)} %all-gather.22.cloned.1.call-done), kind=kOutput, calls=%fused_computation.10 | convolution fusion | flops 1075838976 | bytes 8912896 | tf_op jit(solution)/shard_map/dot_general | solution.py:350
  523.9 8.7 %reduce-scatter.2.cloned.1.call-done = bf16[256,2048]{1,0:T(8,128)(2,1)} async-done(((bf16[512,2048]{1,0:T(8,128)(2,1)}), bf16[256,2048]{1,0:T(8,128)(2,1)}) %reduce-scatter.2.cloned.1.call-update) | async-done | bytes 1048592 | tf_op jit(solution)/shard_map/reduce_scatter | solution.py:348
  (176 shorter events, 60.9 us)
Async XLA Ops:
  6.5 6.9 %copy-start = (bf16[2048,16]{0,1:T(8,128)(2,1)S(1)}, bf16[2048,16]{0,1:T(8,128)(2,1)}, u32[]{:S(2)}) copy-start(bf16[2048,16]{0,1:T(8,128)(2,1)} %param.25) | copy-start | bytes 196612
  6.5 6.4 %copy-start.3 = (bf16[512,2048]{1,0:T(8,128)(2,1)S(1)}, bf16[512,2048]{1,0:T(8,128)(2,1)}, u32[]{:S(2)}) copy-start(bf16[512,2048]{1,0:T(8,128)(2,1)} %param.19) | copy-start | bytes 6291460
  6.5 50.8 %all-gather.24.cloned.1.call-start = ((), (), s32[]{:S(2)}) async-start(), calls=%async_computation.6 | async-start | bytes 2621440 | tf_op jit(solution)/shard_map/all_gather | solution.py:241
  7.3 96.2 %all-gather.18.cloned.1.call-start = ((), (), s32[]{:S(2)}) async-start(), calls=%async_computation.3 | async-start | bytes 2621440 | tf_op jit(solution)/shard_map/all_gather | solution.py:239
  8.0 141.5 %all-gather.16.cloned.1.call-start = ((), (), s32[]{:S(2)}) async-start(), calls=%async_computation.2 | async-start | bytes 2621440 | tf_op jit(solution)/shard_map/all_gather | solution.py:238
  8.7 4.7 copy-start.24
  8.8 4.7 copy-start.21
  8.8 4.7 copy-start.22
  8.8 186.6 %all-gather.14.cloned.1.call-start = ((), (), s32[]{:S(2)}) async-start(), calls=%async_computation.1 | async-start | bytes 2621440 | tf_op jit(solution)/shard_map/all_gather | solution.py:237
  9.4 240.6 %all-gather.26.cloned.1.call-start = ((), (), s32[]{:S(2)}) async-start(), calls=%async_computation.7 | async-start | bytes 2621440 | tf_op jit(solution)/shard_map/all_gather | solution.py:242
  9.9 324.9 %all-gather.20.cloned.1.call-start = ((), (), s32[]{:S(2)}) async-start(), calls=%async_computation.4 | async-start | bytes 2621440 | tf_op jit(solution)/shard_map/all_gather | solution.py:236
  10.5 381.2 %all-gather.28.cloned.1.call-start = ((), (), s32[]{:S(2)}) async-start(), calls=%async_computation.8 | async-start | bytes 5242880 | tf_op jit(solution)/shard_map/all_gather | solution.py:240
  11.3 461.3 %all-gather.30.cloned.1.call-start = ((), (), s32[]{:S(2)}) async-start(), calls=%async_computation.9 | async-start | bytes 5242880 | tf_op jit(solution)/shard_map/all_gather | solution.py:244
  12.0 506.4 %all-gather.22.cloned.1.call-start = ((), (), s32[]{:S(2)}) async-start(), calls=%async_computation.5 | async-start | bytes 2621440 | tf_op jit(solution)/shard_map/all_gather | solution.py:243
  12.8 519.8 %reduce-scatter.2.cloned.1.call-start = ((), (), s32[]{:S(2)}) async-start(), calls=%async_computation.10 | async-start | bytes 3145728 | tf_op jit(solution)/shard_map/reduce_scatter | solution.py:348
  20.1 37.3 %copy-start.4 = (bf16[512,2048]{1,0:T(8,128)(2,1)S(1)}, bf16[512,2048]{1,0:T(8,128)(2,1)}, u32[]{:S(2)}) copy-start(bf16[512,2048]{1,0:T(8,128)(2,1)} %param.19) | copy-start | bytes 6291460
  40.1 63.3 %copy-start.17 = (f32[512]{0:T(512)S(1)}, f32[512]{0:T(512)}, u32[]{:S(2)}) copy-start(f32[512]{0:T(512)} %copy-done.16) | copy-start | bytes 6148
  40.1 63.3 %copy-start.23 = (f32[2048]{0:T(1024)S(1)}, f32[2048]{0:T(1024)}, u32[]{:S(2)}) copy-start(f32[2048]{0:T(1024)} %param.20) | copy-start | bytes 24580
  200.2 61.6 %collective-permute-start = (bf16[2,1536]{0,1:T(8,128)(2,1)}, bf16[2,1536]{0,1:T(8,128)(2,1)}, u32[]{:S(2)}, u32[]{:S(2)}) collective-permute-start(bf16[2,1536]{0,1:T(8,128)(2,1)} %get-tuple-element.20), channel_id=1, source_target_pairs={{0,8},{8,16},{16,24},{1,9},{9,17},{17,25},{2,10},{10,18},{18,26},{... | collective-permute-start | bytes 18440 | tf_op jit(solution)/shard_map/ppermute | solution.py:21
  203.0 58.8 %collective-permute-start.1 = (bf16[2,1536]{0,1:T(8,128)(2,1)}, bf16[2,1536]{0,1:T(8,128)(2,1)}, u32[]{:S(2)}, u32[]{:S(2)}) collective-permute-start(bf16[2,1536]{0,1:T(8,128)(2,1)} %get-tuple-element.21), channel_id=1, source_target_pairs={{8,0},{16,8},{24,16},{9,1},{17,9},{25,17},{10,2},{18,10},{26,18},{... | collective-permute-start | bytes 18440 | tf_op jit(solution)/shard_map/ppermute | solution.py:23
  255.4 83.5 %collective-permute-start.2 = (bf16[128,1024]{0,1:T(8,128)(2,1)}, bf16[128,1024]{0,1:T(8,128)(2,1)S(1)}, u32[]{:S(2)}, u32[]{:S(2)}) collective-permute-start(bf16[128,1024]{0,1:T(8,128)(2,1)} %get-tuple-element.37), channel_id=1, source_target_pairs={{0,8},{8,16},{16,24},{1,9},{9,17},{17,25},{2,10},{10,18},{18,26},{... | collective-permute-start | bytes 786440 | tf_op jit(solution)/shard_map/ppermute | solution.py:21
  257.4 81.5 %collective-permute-start.3 = (bf16[128,1024]{0,1:T(8,128)(2,1)}, bf16[128,1024]{0,1:T(8,128)(2,1)}, u32[]{:S(2)}, u32[]{:S(2)}) collective-permute-start(bf16[128,1024]{0,1:T(8,128)(2,1)} %get-tuple-element.38), channel_id=1, source_target_pairs={{8,0},{16,8},{24,16},{9,1},{17,9},{25,17},{10,2},{18,10},{26,18},{... | collective-permute-start | bytes 786440 | tf_op jit(solution)/shard_map/ppermute | solution.py:23
  273.5 3.8 copy-start.2
  282.8 41.7 %copy-start.6 = (f32[4,4,128,128]{3,2,1,0:T(8,128)S(1)}, f32[4,4,128,128]{3,2,1,0:T(8,128)}, u32[]{:S(2)}) copy-start(f32[4,4,128,128]{3,2,1,0:T(8,128)} %fusion.56) | copy-start | bytes 3145732
  282.9 41.7 %copy-start.12 = (f32[4,4,2,128]{3,2,1,0:T(2,128)S(1)}, f32[4,4,2,128]{3,2,1,0:T(2,128)}, u32[]{:S(2)}) copy-start(f32[4,4,2,128]{3,2,1,0:T(2,128)} %copy.184) | copy-start | bytes 49156
  308.5 17.8 %copy-start.14 = (f32[4,4,2]{0,2,1:T(2,128)S(1)}, f32[4,4,2]{0,2,1:T(2,128)}, u32[]{:S(2)}) copy-start(f32[4,4,2]{0,2,1:T(2,128)} %copy.195) | copy-start | bytes 388
  308.5 17.8 %copy-start.20 = (pred[4,4]{1,0:T(4,128)(4,1)S(1)}, pred[4,4]{1,0:T(4,128)(4,1)}, u32[]{:S(2)}) copy-start(pred[4,4]{1,0:T(4,128)(4,1)} %iota_compare_fusion.1) | copy-start | bytes 52
  326.2 3.9 copy-start.13
  326.3 3.9 copy-start.19
  334.8 3.9 copy-start.15
  401.7 6.7 %copy-start.5 = (f32[4,128,4,2,128]{4,3,2,1,0:T(2,128)S(1)}, f32[4,128,4,2,128]{4,3,2,1,0:T(2,128)}, u32[]{:S(2)}) copy-start(f32[4,128,4,2,128]{4,3,2,1,0:T(2,128)} %reshape.412) | copy-start | bytes 6291460
  518.4 14.2 %copy-start.1 = (bf16[2048,16]{0,1:T(8,128)(2,1)S(1)}, bf16[2048,16]{0,1:T(8,128)(2,1)}, u32[]{:S(2)}) copy-start(bf16[2048,16]{0,1:T(8,128)(2,1)} %param.25) | copy-start | bytes 196612
  (7 other events, 16.8 us)
Sparse Core Ops, SparseCore 0:
  8.9 48.4 all-gather.23
  58.9 44.4 all-gather.17
  105.0 44.4 all-gather.15
  150.9 44.4 all-gather.13
  196.8 53.0 all-gather.25
  251.3 58.3 all-gather.19
  311.3 80.3 all-gather.27
  393.3 79.2 all-gather.29
  474.2 44.1 all-gather.21
  524.0 8.5 reduce-scatter.1
where the time goes:
time: 549 us; the launch traced here: 540 us
  waiting for transfers between devices  341 us (62%)
  matrix products  60.4 us (11%)
  blocking collectives  52.7 us (10%)
  local copies, waits for them, and re-layouts  33.6 us (6%)
  other arithmetic  28.8 us (5%)
  between operations  14.7 us (3%)
  starting transfers between devices  8.28 us (2%)
    all_gather x1, waiting for transfers between devices, shards(): lax.all_gather(window_output, 'sp', axis=1, tiled=True)  52.7 us
    all_gather x1, waiting for transfers between devices, shards(): lax.all_gather(window_query, 'sp', axis=0, tiled=True)  45.2 us
    all_gather x1, waiting for transfers between devices, shards(): lax.all_gather(window_values, 'sp', axis=0, tiled=True)  44.7 us
    all_gather x1, waiting for transfers between devices, shards(): lax.all_gather(state_query, 'sp', axis=0, tiled=True)  43 us
    all_gather x1, waiting for transfers between devices, shards(): lax.all_gather(state_keys, 'sp', axis=0, tiled=True)  42.5 us
    all_gather x1, waiting for transfers between devices, shards(): lax.all_gather(state_value, 'sp', axis=0, tiled=True)  42.3 us
    all_gather x1, waiting for transfers between devices, shards(): lax.all_gather(state_output, 'sp', axis=1, tiled=True)  39.2 us
    dot_general x7, matrix products, shards(): jnp.dot(normed, matrix, preferred_element_type=jnp.float32)  26.7 us
  transfers between devices with their start and end apart: 14, of which 9 were waited for; matrix products, arithmetic and copies ran while one was open for 22% of the time, Pallas kernels for 0%

commit v1 on v0

--- a/solution.py
+++ b/solution.py
@@ -8,6 +8,28 @@
 WINDOW = 128
 BLOCK = 128
 GRID_WIDTH = 64
+
+
+def joined_along(blocks, dim):
+    blocks = jnp.moveaxis(blocks, 0, dim)
+    shape = blocks.shape
+    return blocks.reshape(*shape[:dim], shape[dim] * shape[dim + 1], *shape[dim + 2 :])
+
+
+def collected_by_bits(shard, axis):
+    devices = lax.axis_size(axis)
+    blocks = shard[None]
+    for level in range(devices.bit_length() - 1):
+        stride = 1 << level
+        other = lax.ppermute(blocks, axis, [(i, i ^ stride) for i in range(devices)])
+        both = jnp.stack([blocks, other])
+        upper = lax.axis_index(axis) >> level & 1
+        blocks = jnp.where(upper == 0, both, both[::-1]).reshape(-1, *shard.shape)
+    return blocks
+
+
+def collect(x, axis, dim):
+    return joined_along(collected_by_bits(x, axis), dim)
 
 
 def extended(cells, sides, width):
@@ -236,7 +258,7 @@
         lax.all_gather(state_gate, "sp", axis=0, tiled=True),
         lax.all_gather(state_value, "sp", axis=0, tiled=True),
         lax.all_gather(state_keys, "sp", axis=0, tiled=True),
-        lax.all_gather(state_query, "sp", axis=0, tiled=True),
+        collect(state_query, "sp", 0),
         lax.all_gather(window_query, "sp", axis=0, tiled=True),
         lax.all_gather(window_keys, "sp", axis=0, tiled=True),
         lax.all_gather(window_values, "sp", axis=0, tiled=True),

time: 549 us -> 530 us (0.965); the launches traced: 540 us -> 527 us
  waiting for transfers between devices: 341 us -> 301 us
  blocking collectives: 52.7 us -> 73.7 us
    ppermute x0 -> x2, waiting for transfers between devices: none -> 73.2 us  [collected_by_bits(): lax.ppermute(blocks, axis, [(i, i ^ stride) for i in range(devices)])]
    all_gather x1 -> x0, waiting for transfers between devices: 43 us -> none  [shards(): lax.all_gather(state_query, 'sp', axis=0, tiled=True)]
    all_gather x1, waiting for transfers between devices: 42.5 us -> 0.02 us  [shards(): lax.all_gather(state_keys, 'sp', axis=0, tiled=True)]
    all_gather x1, blocking collectives: 13.3 us -> 34.2 us  [shards(): lax.all_gather(overall[None].astype(jnp.bfloat16), 'sp', axis=0, tiled=True)]
    all_gather x1, waiting for transfers between devices: 17.2 us -> 0.02 us  [shards(): lax.all_gather(window_keys, 'sp', axis=0, tiled=True)]
    all_gather x1, waiting for transfers between devices: 42.3 us -> 32.2 us  [shards(): lax.all_gather(state_value, 'sp', axis=0, tiled=True)]
  transfers between devices with their start and end apart: 14 -> 15, of which waited for: 9 -> 7; matrix products, arithmetic and copies ran while one was open for 22% -> 23% of each run, Pallas kernels for 0% -> 0%
where the time goes in v1:
time: 530 us; the launch traced here: 527 us
  waiting for transfers between devices  301 us (57%)
  blocking collectives  73.7 us (14%)
  matrix products  58.8 us (11%)
  local copies, waits for them, and re-layouts  34.9 us (7%)
  other arithmetic  32.4 us (6%)
  between operations  14.4 us (3%)
  starting transfers between devices  11.4 us (2%)
    ppermute x2, waiting for transfers between devices, collected_by_bits(): lax.ppermute(blocks, axis, [(i, i ^ stride) for i in range(devices)])  73.2 us
    all_gather x1, waiting for transfers between devices, shards(): lax.all_gather(window_output, 'sp', axis=1, tiled=True)  54.2 us
    all_gather x1, waiting for transfers between devices, shards(): lax.all_gather(window_values, 'sp', axis=0, tiled=True)  44.6 us
    all_gather x1, waiting for transfers between devices, shards(): lax.all_gather(window_query, 'sp', axis=0, tiled=True)  44.4 us
    all_gather x1, waiting for transfers between devices, shards(): lax.all_gather(state_output, 'sp', axis=1, tiled=True)  39.2 us
    all_gather x1, blocking collectives, shards(): lax.all_gather(overall[None].astype(jnp.bfloat16), 'sp', axis=0, tiled=True)  34.2 us
    all_gather x1, waiting for transfers between devices, shards(): lax.all_gather(state_value, 'sp', axis=0, tiled=True)  32.2 us
    dot_general x7, matrix products, shards(): jnp.dot(normed, matrix, preferred_element_type=jnp.float32)  25.1 us
  transfers between devices with their start and end apart: 15, of which 7 were waited for; matrix products, arithmetic and copies ran while one was open for 23% of the time, Pallas kernels for 0%

profile of v1, /device:TPU:0, one launch (start us, length us, event | category | flops | bytes accessed | tf_op | source)
XLA Modules:
  0.0 526.5 jit_solution(4646906267845557826)
XLA Ops:
  11.3 3.1 collective-permute-start
  18.5 34.2 %all-gather.3 = bf16[4,4,2]{1,2,0:T(2,128)(2,1)S(1)} all-gather(bf16[1,4,2]{1,2,0:T(2,128)(2,1)S(1)} %convert_bitcast_fusion), channel_id=2, replica_groups=mesh['sp'=4,'fs'=4,'tp'=2] {'sp'}, dimensions={0}, use_global_device_ids=true | all-gather | bytes 80 | tf_op jit(solution)/shard_map/all_gather | solution.py:330
  65.2 73.2 %collective-permute-done.1 = bf16[2,512,512]{2,1,0:T(8,128)(2,1)} collective-permute-done((bf16[2,512,512]{2,1,0:T(8,128)(2,1)}, bf16[2,512,512]{2,1,0:T(8,128)(2,1)}, u32[]{:S(2)}, u32[]{:S(2)}) %collective-permute-start.1) | collective-permute-done | bytes 1048608 | tf_op jit(solution)/shard_map/ppermute | solution.py:24
  142.9 3.9 convolution_convert_fusion.2
  146.9 3.6 convolution_convert_fusion.5
  150.5 32.2 %all-gather.13.cloned.1.call-done = bf16[2048,512]{1,0:T(8,128)(2,1)} async-done(((bf16[512,512]{1,0:T(8,128)(2,1)}), bf16[2048,512]{1,0:T(8,128)(2,1)}) %all-gather.13.cloned.1.call-update) | async-done | bytes 2097168 | tf_op jit(solution)/shard_map/all_gather | solution.py:259
  182.7 3.6 convolution_convert_fusion.6
  187.5 2.8 collective-permute-start.2
  190.3 1.9 collective-permute-start.3
  192.5 44.6 %all-gather.23.cloned.1.call-done = bf16[2048,512]{1,0:T(8,128)(2,1)} async-done(((bf16[512,512]{1,0:T(8,128)(2,1)}), bf16[2048,512]{1,0:T(8,128)(2,1)}) %all-gather.23.cloned.1.call-update) | async-done | bytes 2097168 | tf_op jit(solution)/shard_map/all_gather | solution.py:264
  237.2 3.6 convolution_convert_fusion.1
  242.7 2.0 collective-permute-start.4
  246.0 2.1 copy.213
  249.1 5.9 %maximum_maximum_fusion = (bf16[514,1536]{0,1:T(8,128)(2,1)S(1)}, bf16[514,1536]{0,1:T(8,128)(2,1)S(1)}) fusion(bf16[512,512]{0,1:T(8,128)(2,1)S(1)} %convolution_convert_fusion.4, bf16[512,512]{0,1:T(8,128)(2,1)S(1)} %convolution_convert_fusion.5, bf16[512,512]{0,1:T(8,128)(2,1)S(1)} %convolution_convert_fusion.6, ...), kind=kLoop, calls=%fused_computation.21 | loop fusion | flops 12632064 | bytes 4743168 | tf_op jit(solution)/shard_map/concatenate | solution.py:41
  255.0 5.8 %fusion.124 = (bf16[512,1536]{0,1:T(8,128)(2,1)}, f32[512,1536]{0,1:T(8,128)S(1)}) fusion(f32[1536]{0:T(1024)S(1)} %copy-done.17, bf16[514,1536]{0,1:T(8,128)(2,1)S(1)} %get-tuple-element.19, f32[1536]{0:T(1024)S(1)} %copy-done.14, f32[1536]{0:T(1024)S(1)} %copy-done.15, bf16[512,512]{0,1:T(8,128)(2,1)S(1)} %convolution_convert_fusion.4, ...), kind=kLoop, calls=%fused_computation.227 | loop fusion | flops 15728640 | bytes 12613632 | tf_op jit(solution)/shard_map/convert.2
  262.1 2.6 reshape.413
  271.4 23.5 %all-gather.1 = bf16[16,2,128,64]{2,3,1,0:T(8,128)(2,1)S(1)} all-gather(bf16[4,2,128,64]{2,3,1,0:T(8,128)(2,1)S(1)} %get-tuple-element.61), channel_id=3, replica_groups=mesh['sp'=4,'fs'=4,'tp'=2] {'sp'}, dimensions={0}, use_global_device_ids=true | all-gather | bytes 655360 | tf_op jit(solution)/shard_map/all_gather | solution.py:324
  296.0 16.0 %all-gather.2 = bf16[16,2,128,64]{2,3,1,0:T(8,128)(2,1)S(1)} all-gather(bf16[4,2,128,64]{2,3,1,0:T(8,128)(2,1)S(1)} %get-tuple-element.64), channel_id=4, replica_groups=mesh['sp'=4,'fs'=4,'tp'=2] {'sp'}, dimensions={0}, use_global_device_ids=true | all-gather | bytes 655360 | tf_op jit(solution)/shard_map/all_gather | solution.py:327
  313.8 2.6 fusion.20
  317.7 2.7 fusion.19
  323.3 3.5 bitcast_reduce_fusion
  327.1 2.0 pad_maximum_fusion.9
  334.7 44.4 %all-gather.25.cloned.1.call-done = bf16[2048,1024]{1,0:T(8,128)(2,1)} async-done(((bf16[512,1024]{1,0:T(8,128)(2,1)}), bf16[2048,1024]{1,0:T(8,128)(2,1)}) %all-gather.25.cloned.1.call-update) | async-done | bytes 4194320 | tf_op jit(solution)/shard_map/all_gather | solution.py:262
  379.1 5.4 %convolution_convert_fusion = bf16[512,1024]{1,0:T(8,128)(2,1)S(1)} fusion(bf16[2048,1024]{1,0:T(8,128)(2,1)} %all-gather.25.cloned.1.call-done, bf16[512,2048]{1,0:T(8,128)(2,1)} %param.19, f32[2048]{0:T(1024)S(1)} %copy-done.33, f32[512]{0:T(512)S(1)} %copy-done.27), kind=kOutput, calls=%fused_computation.37 | convolution fusion | flops 2152202240 | bytes 7350272 | tf_op jit(solution)/shard_map/dot_general | solution.py:269
  384.5 3.1 reshape.416
  394.1 5.4 %fusion = (f32[4,4,2,128]{3,2,1,0:T(2,128)S(1)}, f32[4,4,384,128,2]{3,2,4,1,0:T(8,128)S(1)}) fusion(pred[4,128,384]{1,2,0:T(8,128)(4,1)S(1)} %copy-done.9, f32[4,128,4,2,128]{4,3,2,1,0:T(2,128)S(1)} %copy-done.7, bf16[4,128,4,2,32]{4,1,3,2,0:T(8,128)(2,1)} %copy.223, bf16[4,128,4,2,32]{4,1,3,2,0:T(8,128)(2,1)} %copy.222, ...), kind=kOutput, calls=%fused_computation.3 | convolution fusion | flops 418377728 | bytes 11747328 | tf_op jit(solution)/shard_map/kihgd,kjhd->khgij/dot_general | solution.py:88
  401.4 2.3 fusion.18
  405.6 54.2 %all-gather.27.cloned.1.call-done = bf16[1024,2048]{1,0:T(8,128)(2,1)} async-done(((bf16[1024,512]{1,0:T(8,128)(2,1)}), bf16[1024,2048]{1,0:T(8,128)(2,1)}) %all-gather.27.cloned.1.call-update) | async-done | bytes 4194320 | tf_op jit(solution)/shard_map/all_gather | solution.py:266
  459.8 6.6 %fusion.130 = f32[512,2048]{1,0:T(8,128)} fusion(bf16[512,1024]{1,0:T(8,128)(2,1)S(1)} %convert_element_type.224, bf16[1024,2048]{1,0:T(8,128)(2,1)} %all-gather.27.cloned.1.call-done), kind=kOutput, calls=%fused_computation.233 | convolution fusion | flops 2147483648 | bytes 9437184 | tf_op jit(solution)/shard_map/dot_general | solution.py:373
  466.3 39.2 %all-gather.19.cloned.1.call-done = bf16[512,2048]{1,0:T(8,128)(2,1)} async-done(((bf16[512,512]{1,0:T(8,128)(2,1)}), bf16[512,2048]{1,0:T(8,128)(2,1)}) %all-gather.19.cloned.1.call-update) | async-done | bytes 2097168 | tf_op jit(solution)/shard_map/all_gather | solution.py:265
  505.5 5.5 %add_convert_fusion = bf16[512,2048]{1,0:T(8,128)(2,1)} fusion(f32[512,2048]{1,0:T(8,128)} %fusion.130, bf16[512,512]{0,1:T(8,128)(2,1)S(1)} %fusion.41, bf16[512,2048]{1,0:T(8,128)(2,1)} %all-gather.19.cloned.1.call-done), kind=kOutput, calls=%fused_computation.10 | convolution fusion | flops 1075838976 | bytes 8912896 | tf_op jit(solution)/shard_map/dot_general | solution.py:372
  511.0 8.7 %reduce-scatter.2.cloned.1.call-done = bf16[256,2048]{1,0:T(8,128)(2,1)} async-done(((bf16[512,2048]{1,0:T(8,128)(2,1)}), bf16[256,2048]{1,0:T(8,128)(2,1)}) %reduce-scatter.2.cloned.1.call-update) | async-done | bytes 1048592 | tf_op jit(solution)/shard_map/reduce_scatter | solution.py:370
  (201 shorter events, 62.0 us)
Async XLA Ops:
  6.5 9.7 %copy-start = (bf16[2048,16]{0,1:T(8,128)(2,1)S(1)}, bf16[2048,16]{0,1:T(8,128)(2,1)}, u32[]{:S(2)}) copy-start(bf16[2048,16]{0,1:T(8,128)(2,1)} %param.25) | copy-start | bytes 196612
  6.5 136.4 %all-gather.21.cloned.1.call-start = ((), (), s32[]{:S(2)}) async-start(), calls=%async_computation.5 | async-start | bytes 2621440 | tf_op jit(solution)/shard_map/all_gather | solution.py:263
  7.3 139.6 %all-gather.15.cloned.1.call-start = ((), (), s32[]{:S(2)}) async-start(), calls=%async_computation.2 | async-start | bytes 2621440 | tf_op jit(solution)/shard_map/all_gather | solution.py:260
  8.0 7.7 %copy-start.4 = (bf16[512,2048]{1,0:T(8,128)(2,1)S(1)}, bf16[512,2048]{1,0:T(8,128)(2,1)}, u32[]{:S(2)}) copy-start(bf16[512,2048]{1,0:T(8,128)(2,1)} %param.19) | copy-start | bytes 6291460
  8.0 174.6 %all-gather.13.cloned.1.call-start = ((), (), s32[]{:S(2)}) async-start(), calls=%async_computation.1 | async-start | bytes 2621440 | tf_op jit(solution)/shard_map/all_gather | solution.py:259
  8.8 228.4 %all-gather.23.cloned.1.call-start = ((), (), s32[]{:S(2)}) async-start(), calls=%async_computation.6 | async-start | bytes 2621440 | tf_op jit(solution)/shard_map/all_gather | solution.py:264
  9.3 313.9 %all-gather.17.cloned.1.call-start = ((), (), s32[]{:S(2)}) async-start(), calls=%async_computation.3 | async-start | bytes 2621440 | tf_op jit(solution)/shard_map/all_gather | solution.py:258
  9.9 369.2 %all-gather.25.cloned.1.call-start = ((), (), s32[]{:S(2)}) async-start(), calls=%async_computation.7 | async-start | bytes 5242880 | tf_op jit(solution)/shard_map/all_gather | solution.py:262
  10.5 5.7 %copy-start.34 = (f32[8]{0:T(128)S(1)}, f32[8]{0:T(128)}, u32[]{:S(2)}) copy-start(f32[8]{0:T(128)} %param.26) | copy-start | bytes 100
  10.5 5.7 %copy-start.31 = (f32[512,8]{0,1:T(8,128)S(1)}, f32[512,8]{0,1:T(8,128)}, u32[]{:S(2)}) copy-start(f32[512,8]{0,1:T(8,128)} %param.27) | copy-start | bytes 49156
  10.5 5.7 %copy-start.32 = (f32[2048]{0:T(1024)S(1)}, f32[2048]{0:T(1024)}, u32[]{:S(2)}) copy-start(f32[2048]{0:T(1024)} %param.20) | copy-start | bytes 24580
  10.5 449.2 %all-gather.27.cloned.1.call-start = ((), (), s32[]{:S(2)}) async-start(), calls=%async_computation.8 | async-start | bytes 5242880 | tf_op jit(solution)/shard_map/all_gather | solution.py:266
  11.3 494.2 %all-gather.19.cloned.1.call-start = ((), (), s32[]{:S(2)}) async-start(), calls=%async_computation.4 | async-start | bytes 2621440 | tf_op jit(solution)/shard_map/all_gather | solution.py:265
  11.3 44.2 %collective-permute-start = (bf16[1,512,512]{2,1,0:T(8,128)(2,1)}, bf16[1,512,512]{2,1,0:T(8,128)(2,1)}, u32[]{:S(2)}, u32[]{:S(2)}) collective-permute-start(bf16[1,512,512]{2,1,0:T(8,128)(2,1)} %bitcast.9), channel_id=1, source_target_pairs={{0,8},{8,0},{16,24},{24,16},{1,9},{9,1},{17,25},{25,17},{2,10},{10... | collective-permute-start | bytes 1572872 | tf_op jit(solution)/shard_map/ppermute | solution.py:24
  14.5 505.3 %reduce-scatter.2.cloned.1.call-start = ((), (), s32[]{:S(2)}) async-start(), calls=%async_computation.9 | async-start | bytes 3145728 | tf_op jit(solution)/shard_map/reduce_scatter | solution.py:370
  16.2 221.0 %copy-start.26 = (f32[512]{0:T(512)}, f32[512]{0:T(512)S(1)}, u32[]{:S(2)}) copy-start(f32[512]{0:T(512)S(1)} %add_rsqrt_fusion.1) | copy-start | bytes 6148
  58.5 3.9 copy-start.23
  58.5 3.9 copy-start.24
  58.5 80.0 %collective-permute-start.1 = (bf16[2,512,512]{2,1,0:T(8,128)(2,1)}, bf16[2,512,512]{2,1,0:T(8,128)(2,1)}, u32[]{:S(2)}, u32[]{:S(2)}) collective-permute-start(bf16[2,512,512]{2,1,0:T(8,128)(2,1)} %get-tuple-element.32), channel_id=1, source_target_pairs={{0,16},{8,24},{16,0},{24,8},{1,17},{9,25},{17,1},{25,9},{2,18},{10... | collective-permute-start | bytes 3145736 | tf_op jit(solution)/shard_map/ppermute | solution.py:24
  59.7 78.7 %copy-start.3 = (bf16[1,2,512,512]{3,2,1,0:T(8,128)(2,1)S(1)}, bf16[1,2,512,512]{3,2,1,0:T(8,128)(2,1)}, u32[]{:S(2)}) copy-start(bf16[1,2,512,512]{3,2,1,0:T(8,128)(2,1)} %get-tuple-element.31) | copy-start | bytes 3145732
  187.5 61.6 %collective-permute-start.2 = (bf16[2,1536]{0,1:T(8,128)(2,1)}, bf16[2,1536]{0,1:T(8,128)(2,1)}, u32[]{:S(2)}, u32[]{:S(2)}) collective-permute-start(bf16[2,1536]{0,1:T(8,128)(2,1)} %get-tuple-element.20), channel_id=1, source_target_pairs={{0,8},{8,16},{16,24},{1,9},{9,17},{17,25},{2,10},{10,18},{18,26},{... | collective-permute-start | bytes 18440 | tf_op jit(solution)/shard_map/ppermute | solution.py:43
  190.3 58.8 %collective-permute-start.3 = (bf16[2,1536]{0,1:T(8,128)(2,1)}, bf16[2,1536]{0,1:T(8,128)(2,1)}, u32[]{:S(2)}, u32[]{:S(2)}) collective-permute-start(bf16[2,1536]{0,1:T(8,128)(2,1)} %get-tuple-element.21), channel_id=1, source_target_pairs={{8,0},{16,8},{24,16},{9,1},{17,9},{25,17},{10,2},{18,10},{26,18},{... | collective-permute-start | bytes 18440 | tf_op jit(solution)/shard_map/ppermute | solution.py:45
  242.7 84.4 %collective-permute-start.4 = (bf16[128,1024]{0,1:T(8,128)(2,1)}, bf16[128,1024]{0,1:T(8,128)(2,1)S(1)}, u32[]{:S(2)}, u32[]{:S(2)}) collective-permute-start(bf16[128,1024]{0,1:T(8,128)(2,1)} %get-tuple-element.39), channel_id=1, source_target_pairs={{0,8},{8,16},{16,24},{1,9},{9,17},{17,25},{2,10},{10,18},{18,26},{... | collective-permute-start | bytes 786440 | tf_op jit(solution)/shard_map/ppermute | solution.py:43
  244.7 82.3 %collective-permute-start.5 = (bf16[128,1024]{0,1:T(8,128)(2,1)}, bf16[128,1024]{0,1:T(8,128)(2,1)}, u32[]{:S(2)}, u32[]{:S(2)}) collective-permute-start(bf16[128,1024]{0,1:T(8,128)(2,1)} %get-tuple-element.40), channel_id=1, source_target_pairs={{8,0},{16,8},{24,16},{9,1},{17,9},{25,17},{10,2},{18,10},{26,18},{... | collective-permute-start | bytes 786440 | tf_op jit(solution)/shard_map/ppermute | solution.py:45
  249.0 6.0 %copy-start.13 = (f32[1536]{0:T(1024)S(1)}, f32[1536]{0:T(1024)}, u32[]{:S(2)}) copy-start(f32[1536]{0:T(1024)} %get-tuple-element.5) | copy-start | bytes 18436
  249.0 6.0 %copy-start.14 = (f32[1536]{0:T(1024)S(1)}, f32[1536]{0:T(1024)}, u32[]{:S(2)}) copy-start(f32[1536]{0:T(1024)} %get-tuple-element.6) | copy-start | bytes 18436
  249.0 6.0 %copy-start.15 = (f32[1536]{0:T(1024)S(1)}, f32[1536]{0:T(1024)}, u32[]{:S(2)}) copy-start(f32[1536]{0:T(1024)} %get-tuple-element.7) | copy-start | bytes 18436
  249.0 6.0 %copy-start.16 = (f32[1536]{0:T(1024)S(1)}, f32[1536]{0:T(1024)}, u32[]{:S(2)}) copy-start(f32[1536]{0:T(1024)} %get-tuple-element.8) | copy-start | bytes 18436
  249.0 6.0 %copy-start.17 = (f32[1536]{0:T(1024)S(1)}, f32[1536]{0:T(1024)}, u32[]{:S(2)}) copy-start(f32[1536]{0:T(1024)} %get-tuple-element.9) | copy-start | bytes 18436
  271.4 40.7 %copy-start.8 = (f32[4,4,128,128]{3,2,1,0:T(8,128)S(1)}, f32[4,4,128,128]{3,2,1,0:T(8,128)}, u32[]{:S(2)}) copy-start(f32[4,4,128,128]{3,2,1,0:T(8,128)} %fusion.58) | copy-start | bytes 3145732
  271.4 40.7 %copy-start.19 = (f32[4,4,2,128]{3,2,1,0:T(2,128)S(1)}, f32[4,4,2,128]{3,2,1,0:T(2,128)}, u32[]{:S(2)}) copy-start(f32[4,4,2,128]{3,2,1,0:T(2,128)} %copy.184) | copy-start | bytes 49156
  505.5 14.2 %copy-start.1 = (bf16[2048,16]{0,1:T(8,128)(2,1)S(1)}, bf16[2048,16]{0,1:T(8,128)(2,1)}, u32[]{:S(2)}) copy-start(bf16[2048,16]{0,1:T(8,128)(2,1)} %param.25) | copy-start | bytes 196612
  (18 other events, 41.6 us)
Sparse Core Ops, SparseCore 0:
  8.9 55.9 all-gather.20
  66.4 70.7 all-gather.14
  138.8 43.7 all-gather.12
  184.1 53.0 all-gather.22
  238.6 58.4 all-gather.16
  298.5 80.5 all-gather.24
  380.7 79.0 all-gather.26
  461.3 44.1 all-gather.18
  511.1 8.5 reduce-scatter.1
